TPU v7x, 32 devices: a whole 2x2x4 slice. The times are simulated.
32 devices in a mesh: rep: 2 (over y), fs: 4 (over z), tp: 4 (over x, core).
Axes of the slice: x: 2, y: 2, z: 4, core: 2. Of those that a mesh axis runs over, the one named last changes fastest.
Arguments:
- stream: bfloat16 [2048, 1536], P(('rep', 'fs')), may hold values from -6 to 6
- mix_pre_gain: float32 [1536], replicated, may hold values from 0.1 to 1.9
- w_outer_gate: bfloat16 [1536, 768], P('fs', 'tp'), may hold values from -0.15625 to 0.15625
- w_inner_gate: bfloat16 [1536, 768], P('fs', 'tp'), may hold values from -0.15625 to 0.15625
- w_value: bfloat16 [1536, 768], P('fs', 'tp'), may hold values from -0.15625 to 0.15625
- mix_taps: float32 [3, 768], P(None, 'tp'), may hold values from -3 to 3
- w_mix_out: bfloat16 [768, 1536], P('tp', 'fs'), may hold values from -0.3125 to 0.3125
- mix_post_gain: float32 [1536], replicated, may hold values from 0.1 to 1.9
- ffn_pre_gain: float32 [1536], replicated, may hold values from 0.1 to 1.9
- w_linear: bfloat16 [1536, 4224], P('fs', 'tp'), may hold values from -0.15625 to 0.15625
- w_gated: bfloat16 [1536, 4224], P('fs', 'tp'), may hold values from -0.15625 to 0.15625
- ffn_taps: float32 [3, 4224], P(None, 'tp'), may hold values from -3 to 3
- ffn_bias: float32 [4224], P('tp'), may hold values from -3 to 3
- w_down: bfloat16 [4224, 1536], P('tp', 'fs'), may hold values from -0.125 to 0.125
- ffn_post_gain: float32 [1536], replicated, may hold values from 0.1 to 1.9
Outputs:
- result: bfloat16 [2048, 1536], P(('rep', 'fs'))
All inputs are finite; a program needn't handle non-finite values.
Results may differ from a plain program's by a relative error of at most 0.023.
Values may be sent and summed in bfloat16 or wider, within the bound.
A program may use at most 64 MiB of HBM per device.

v0:
```python
import jax
import jax.numpy as jnp
from jax import lax
from jax.sharding import PartitionSpec as P

SEQ_LEN = 128
EPS = 1e-06


def norm_scale(values, gain):
    return values * lax.rsqrt(jnp.mean(values * values, axis=-1, keepdims=True) + EPS) * gain


def conv_three(values, taps):
    height, breadth = values.shape
    grouped = values.reshape(height // SEQ_LEN, SEQ_LEN, breadth)
    padded = jnp.pad(grouped, ((0, 0), (1, 1), (0, 0)))
    mixed = taps[0] * padded[:, :-2] + taps[1] * padded[:, 1:-1] + taps[2] * padded[:, 2:]
    return mixed.reshape(height, breadth)


def settle(partial_value, resid, post_gain):
    branch = lax.psum(partial_value.astype(jnp.bfloat16), "tp")
    return (resid + norm_scale(branch.astype(jnp.float32), post_gain)).astype(jnp.bfloat16)


def on_device(
    stream,
    mix_pre_gain,
    w_outer_gate,
    w_inner_gate,
    w_value,
    mix_taps,
    w_mix_out,
    mix_post_gain,
    ffn_pre_gain,
    w_linear,
    w_gated,
    ffn_taps,
    ffn_bias,
    w_down,
    ffn_post_gain,
):
    resid = stream.astype(jnp.float32)
    normed = norm_scale(resid, mix_pre_gain).astype(jnp.bfloat16)
    full_outer, full_inner, full_value = (
        lax.all_gather(w_outer_gate, "fs", axis=0, tiled=True),
        lax.all_gather(w_inner_gate, "fs", axis=0, tiled=True),
        lax.all_gather(w_value, "fs", axis=0, tiled=True),
    )
    outer = jnp.dot(normed, full_outer, preferred_element_type=jnp.float32)
    inner = jnp.dot(normed, full_inner, preferred_element_type=jnp.float32)
    value = jnp.dot(normed, full_value, preferred_element_type=jnp.float32)
    outer = outer.astype(jnp.bfloat16)
    inner = inner.astype(jnp.bfloat16)
    value = value.astype(jnp.bfloat16)
    product = inner.astype(jnp.float32) * value.astype(jnp.float32)
    mixed = (outer.astype(jnp.float32) * conv_three(product, mix_taps)).astype(jnp.bfloat16)
    full_mix_out = lax.all_gather(w_mix_out, "fs", axis=1, tiled=True)
    partial_value = jnp.dot(mixed, full_mix_out, preferred_element_type=jnp.float32)
    middle = settle(partial_value, resid, mix_post_gain)
    middle_f = middle.astype(jnp.float32)
    normed_two = norm_scale(middle_f, ffn_pre_gain).astype(jnp.bfloat16)
    full_linear, full_gated = (
        lax.all_gather(w_linear, "fs", axis=0, tiled=True),
        lax.all_gather(w_gated, "fs", axis=0, tiled=True),
    )
    linear = jnp.dot(normed_two, full_linear, preferred_element_type=jnp.float32)
    gated = jnp.dot(normed_two, full_gated, preferred_element_type=jnp.float32)
    linear = linear.astype(jnp.bfloat16)
    gated = gated.astype(jnp.bfloat16)
    activated = jax.nn.gelu(
        conv_three(gated.astype(jnp.float32), ffn_taps) + ffn_bias, approximate=True
    )
    hidden = (activated * linear.astype(jnp.float32)).astype(jnp.bfloat16)
    full_down = lax.all_gather(w_down, "fs", axis=1, tiled=True)
    partial_two = jnp.dot(hidden, full_down, preferred_element_type=jnp.float32)
    return settle(partial_two, middle_f, ffn_post_gain)


def solution(mesh):
    in_specs = (
        P(("rep", "fs"), None),
        P(),
        P("fs", "tp"),
        P("fs", "tp"),
        P("fs", "tp"),
        P(None, "tp"),
        P("tp", "fs"),
        P(),
        P(),
        P("fs", "tp"),
        P("fs", "tp"),
        P(None, "tp"),
        P("tp"),
        P("tp", "fs"),
        P(),
    )
    out_specs = P(("rep", "fs"), None)
    return jax.shard_map(
        on_device, mesh=mesh, in_specs=in_specs, out_specs=out_specs, check_vma=False
    )
```

profile of v0, /device:TPU:0, one launch (start us, length us, event | category | flops | bytes accessed | tf_op | source)
XLA Modules:
  0.0 331.4 jit_solution(645357725762932306)
XLA Ops:
  7.4 1.5 fusion.8
  8.8 18.7 %all_gather.22 = bf16[1536,192]{0,1:T(8,128)(2,1)S(1)} all-gather(bf16[384,192]{0,1:T(8,128)(2,1)} %param.18), channel_id=1, replica_groups=mesh['rep'=2,'fs'=4,'tp'=4] {'fs'}, dimensions={0}, use_global_device_ids=true | all-gather | bytes 737280 | tf_op jit(solution)/shard_map/all_gather | solution.py:48
  27.5 16.1 %all_gather.23 = bf16[1536,192]{0,1:T(8,128)(2,1)S(1)} all-gather(bf16[384,192]{0,1:T(8,128)(2,1)S(1)} %copy-done.1), channel_id=1, replica_groups=mesh['rep'=2,'fs'=4,'tp'=4] {'fs'}, dimensions={0}, use_global_device_ids=true | all-gather | bytes 737280 | tf_op jit(solution)/shard_map/all_gather | solution.py:49
  43.7 0.5 fusion.18
  44.2 0.5 fusion.17
  44.7 0.1 reshape.58
  44.9 0.0 copy-done.7
  44.9 0.2 copy-done.2
  45.1 16.4 %all_gather.21 = bf16[1536,192]{0,1:T(8,128)(2,1)S(1)} all-gather(bf16[384,192]{0,1:T(8,128)(2,1)S(1)} %copy-done.2), channel_id=1, replica_groups=mesh['rep'=2,'fs'=4,'tp'=4] {'fs'}, dimensions={0}, use_global_device_ids=true | all-gather | bytes 737280 | tf_op jit(solution)/shard_map/all_gather | solution.py:47
  61.5 15.5 %all_gather.24 = bf16[192,1536]{1,0:T(8,128)(2,1)S(1)} all-gather(bf16[192,384]{1,0:T(8,128)(2,1)S(1)} %copy-done.3), channel_id=1, replica_groups=mesh['rep'=2,'fs'=4,'tp'=4] {'fs'}, dimensions={1}, use_global_device_ids=true | all-gather | bytes 737280 | tf_op jit(solution)/shard_map/all_gather | solution.py:59
  77.0 1.2 fusion.43
  78.2 2.1 convolution_convert_fusion.3
  80.4 0.0 all-gather.4.cloned.1.call-start
  80.4 0.5 all-gather.4.cloned.1.call-update
  80.9 0.0 all-gather.6.cloned.1.call-start
  81.0 0.5 all-gather.6.cloned.1.call-update
  81.5 0.0 all-gather.8.cloned.1.call-start
  81.6 0.5 all-gather.8.cloned.1.call-update
  82.1 0.0 all-reduce.7.cloned.1.call-start
  82.2 34.8 %all-reduce.5.cloned.1.call-done = bf16[256,1536]{1,0:T(8,128)(2,1)} async-done(((bf16[256,1536]{1,0:T(8,128)(2,1)}), bf16[256,1536]{1,0:T(8,128)(2,1)}) %all-reduce.5.cloned.1.call-update) | async-done | bytes 786448 | tf_op jit(solution)/shard_map/psum | solution.py:23
  117.0 1.4 fusion.4
  118.4 1.7 fusion.12
  120.1 28.7 %all-gather.4.cloned.1.call-done = bf16[1536,1056]{0,1:T(8,128)(2,1)} async-done(((bf16[384,1056]{0,1:T(8,128)(2,1)}), bf16[1536,1056]{0,1:T(8,128)(2,1)}) %all-gather.4.cloned.1.call-update) | async-done | bytes 3244048 | tf_op jit(solution)/shard_map/all_gather | solution.py:66
  148.7 4.0 %fusion.2 = f32[256,1056]{0,1:T(8,128)} fusion(bf16[1536,1056]{0,1:T(8,128)(2,1)} %all-gather.4.cloned.1.call-done, bf16[256,1536]{1,0:T(8,128)(2,1)S(1)} %get-tuple-element.9, f32[1536]{0:T(1024)S(1)} %copy-done.9, f32[256]{0:T(256)S(1)} %add_rsqrt_fusion.1), kind=kOutput, calls=%fused_computation.4 | convolution fusion | flops 832585728 | bytes 5118976 | tf_op jit(solution)/shard_map/dot_general | solution.py:69
  152.8 1.8 reshape.64
  154.6 7.3 %fusion.31 = f32[2,128,1056]{1,0,2:T(2,128)} fusion(f32[2,128,1056]{1,0,2:T(2,128)S(1)} %reshape.64, f32[1056]{0:T(1024)S(1)} %get-tuple-element.6, f32[1056]{0:T(1024)S(1)} %get-tuple-element.7, f32[1056]{0:T(1024)S(1)} %get-tuple-element.5), kind=kLoop, calls=%fused_computation.51 | loop fusion | flops 1351680 | bytes 2175360 | tf_op jit(solution)/shard_map/add | solution.py:18
  162.0 51.6 %all-gather.6.cloned.1.call-done = bf16[1536,1056]{0,1:T(8,128)(2,1)} async-done(((bf16[384,1056]{0,1:T(8,128)(2,1)}), bf16[1536,1056]{0,1:T(8,128)(2,1)}) %all-gather.6.cloned.1.call-update) | async-done | bytes 3244048 | tf_op jit(solution)/shard_map/all_gather | solution.py:65
  213.5 64.8 %all-gather.8.cloned.1.call-done = bf16[1056,1536]{1,0:T(8,128)(2,1)} async-done(((bf16[1056,384]{1,0:T(8,128)(2,1)}), bf16[1056,1536]{1,0:T(8,128)(2,1)}) %all-gather.8.cloned.1.call-update) | async-done | bytes 3244048 | tf_op jit(solution)/shard_map/all_gather | solution.py:76
  278.3 7.9 %convolution_convert_fusion.2 = bf16[256,1536]{1,0:T(8,128)(2,1)} fusion(bf16[1056,1536]{1,0:T(8,128)(2,1)} %all-gather.8.cloned.1.call-done, bf16[1536,1056]{0,1:T(8,128)(2,1)} %all-gather.6.cloned.1.call-done, f32[132,8,2,128]{3,2,1,0:T(2,128)} %bitcast.31, f32[1056]{0:T(1024)S(1)} %copy-done.10, bf16[256,1536]{1,0:T(8,128)(2,1)S(1)} %get-tuple-element.9, ...), kind=kOutput, calls=%fused_computation.6 | convolution fusion | flops 1666424832 | bytes 9153664 | tf_op jit(solution)/shard_map/dot_general | solution.py:77
  286.3 33.8 %all-reduce.7.cloned.1.call-done = bf16[256,1536]{1,0:T(8,128)(2,1)} async-done(((bf16[256,1536]{1,0:T(8,128)(2,1)}), bf16[256,1536]{1,0:T(8,128)(2,1)}) %all-reduce.7.cloned.1.call-update) | async-done | bytes 786448 | tf_op jit(solution)/shard_map/psum | solution.py:23
  320.1 1.4 fusion.6
  321.5 2.4 fusion.15
  (29 shorter events, 0.2 us)
Async XLA Ops:
  7.4 36.3 %copy-start = (bf16[256,1536]{1,0:T(8,128)(2,1)S(1)}, bf16[256,1536]{1,0:T(8,128)(2,1)}, u32[]{:S(2)}) copy-start(bf16[256,1536]{1,0:T(8,128)(2,1)} %param.15) | copy-start | bytes 2359300
  7.4 20.2 %copy-start.1 = (bf16[384,192]{0,1:T(8,128)(2,1)S(1)}, bf16[384,192]{0,1:T(8,128)(2,1)}, u32[]{:S(2)}) copy-start(bf16[384,192]{0,1:T(8,128)(2,1)} %param.19) | copy-start | bytes 442372
  7.4 36.3 %copy-start.8 = (f32[1536]{0:T(1024)S(1)}, f32[1536]{0:T(1024)}, u32[]{:S(2)}) copy-start(f32[1536]{0:T(1024)} %param.16) | copy-start | bytes 18436
  7.4 109.6 %all-reduce.5.cloned.1.call-start = ((), (), s32[]{:S(2)}) async-start(), calls=%async_computation | async-start | bytes 1572864 | tf_op jit(solution)/shard_map/psum | solution.py:23
  44.2 0.7 copy-start.7
  44.2 0.9 copy-start.2
  44.2 17.3 %copy-start.3 = (bf16[192,384]{1,0:T(8,128)(2,1)S(1)}, bf16[192,384]{1,0:T(8,128)(2,1)}, u32[]{:S(2)}) copy-start(bf16[192,384]{1,0:T(8,128)(2,1)} %param.21) | copy-start | bytes 442372
  80.3 1.8 copy-start.4
  80.4 38.0 %copy-start.5 = (f32[1536]{0:T(1024)S(1)}, f32[1536]{0:T(1024)}, u32[]{:S(2)}) copy-start(f32[1536]{0:T(1024)} %param.22) | copy-start | bytes 18436
  80.4 68.4 %all-gather.4.cloned.1.call-start = ((), (), s32[]{:S(2)}) async-start(), calls=%async_computation.1 | async-start | bytes 4055040 | tf_op jit(solution)/shard_map/all_gather | solution.py:66
  80.9 132.6 %all-gather.6.cloned.1.call-start = ((), (), s32[]{:S(2)}) async-start(), calls=%async_computation.2 | async-start | bytes 4055040 | tf_op jit(solution)/shard_map/all_gather | solution.py:65
  81.5 196.8 %all-gather.8.cloned.1.call-start = ((), (), s32[]{:S(2)}) async-start(), calls=%async_computation.3 | async-start | bytes 4055040 | tf_op jit(solution)/shard_map/all_gather | solution.py:76
  82.1 238.0 %all-reduce.7.cloned.1.call-start = ((), (), s32[]{:S(2)}) async-start(), calls=%async_computation.4 | async-start | bytes 1572864 | tf_op jit(solution)/shard_map/psum | solution.py:23
  82.2 66.5 %copy-start.9 = (f32[1536]{0:T(1024)S(1)}, f32[1536]{0:T(1024)}, u32[]{:S(2)}) copy-start(f32[1536]{0:T(1024)} %param.23) | copy-start | bytes 18436
  154.6 123.7 %copy-start.10 = (f32[1056]{0:T(1024)S(1)}, f32[1056]{0:T(1024)}, u32[]{:S(2)}) copy-start(f32[1056]{0:T(1024)} %param.27) | copy-start | bytes 12676
  286.3 35.2 %copy-start.6 = (f32[1536]{0:T(1024)S(1)}, f32[1536]{0:T(1024)}, u32[]{:S(2)}) copy-start(f32[1536]{0:T(1024)} %param.29) | copy-start | bytes 18436
Sparse Core Ops, SparseCore 0:
  80.5 36.4 all-reduce.4
  286.4 33.6 all-reduce.6
Sparse Core Ops, SparseCore 1:
  82.4 66.2 all-gather.3
  150.2 63.3 all-gather.5
  215.0 63.3 all-gather.7
where the time goes:
time: 332 us; the launch traced here: 331 us
  waiting for transfers between devices  215 us (65%)
  blocking collectives  66.7 us (20%)
  other arithmetic  16.8 us (5%)
  between operations  15.2 us (5%)
  matrix products  15.1 us (5%)
    psum x2, waiting for transfers between devices, settle(): branch = lax.psum(partial_value.astype(jnp.bfloat16), 'tp')  68.6 us
    all_gather x1, waiting for transfers between devices, on_device(): full_down = lax.all_gather(w_down, 'fs', axis=1, tiled=True)  64.8 us
    all_gather x1, waiting for transfers between devices, on_device(): lax.all_gather(w_linear, 'fs', axis=0, tiled=True)  51.6 us
    all_gather x1, waiting for transfers between devices, on_device(): lax.all_gather(w_gated, 'fs', axis=0, tiled=True)  28.7 us
    all_gather x1, blocking collectives, on_device(): lax.all_gather(w_inner_gate, 'fs', axis=0, tiled=True)  18.7 us
    all_gather x1, blocking collectives, on_device(): lax.all_gather(w_outer_gate, 'fs', axis=0, tiled=True)  16.4 us
    all_gather x1, blocking collectives, on_device(): lax.all_gather(w_value, 'fs', axis=0, tiled=True)  16.1 us
    all_gather x1, blocking collectives, on_device(): full_mix_out = lax.all_gather(w_mix_out, 'fs', axis=1, tiled=True)  15.5 us
  transfers between devices with their start and end apart: 5, of which 5 were waited for; matrix products, arithmetic and copies ran while one was open for 5% of the time, Pallas kernels for 0%

commit v1 on v0

--- a/solution.py
+++ b/solution.py
@@ -5,6 +5,13 @@
 
 SEQ_LEN = 128
 EPS = 1e-06
+
+
+def swapped_in(x, axis, dim):
+    peers = lax.axis_size(axis)
+    tiles = jnp.stack([x for _ in range(peers)])
+    tiles = lax.all_to_all(tiles, axis, split_axis=0, concat_axis=0)
+    return jnp.concatenate(tiles, axis=dim)
 
 
 def norm_scale(values, gain):
@@ -45,7 +52,7 @@
     normed = norm_scale(resid, mix_pre_gain).astype(jnp.bfloat16)
     full_outer, full_inner, full_value = (
         lax.all_gather(w_outer_gate, "fs", axis=0, tiled=True),
-        lax.all_gather(w_inner_gate, "fs", axis=0, tiled=True),
+        swapped_in(w_inner_gate, "fs", 0),
         lax.all_gather(w_value, "fs", axis=0, tiled=True),
     )
     outer = jnp.dot(normed, full_outer, preferred_element_type=jnp.float32)

time: 332 us -> 332 us (level)
  blocking collectives: 66.7 us -> 60.2 us
  starting transfers between devices: 0.17 us -> 6.65 us
    all_gather x1 -> x0, blocking collectives: 18.7 us -> none  [on_device(): lax.all_gather(w_inner_gate, 'fs', axis=0, tiled=True)]
    all_gather x1, blocking collectives: 16.1 us -> 26.9 us  [on_device(): lax.all_gather(w_value, 'fs', axis=0, tiled=True)]
    all_to_all x0 -> x1, starting transfers between devices: none -> 6.48 us  [swapped_in(): tiles = lax.all_to_all(tiles, axis, split_axis=0, concat_axis=0)]
  transfers between devices with their start and end apart: 5 -> 6, of which waited for: 5 -> 5; matrix products, arithmetic and copies ran while one was open for 5% -> 5% of each run, Pallas kernels for 0% -> 0%
where the time goes in v1:
time: 332 us; the launch traced here: 331 us
  waiting for transfers between devices  215 us (65%)
  blocking collectives  60.2 us (18%)
  other arithmetic  15.5 us (5%)
  between operations  15.2 us (5%)
  matrix products  15.1 us (5%)
  starting transfers between devices  6.65 us (2%)
  local copies, waits for them, and re-layouts  3.94 us (1%)
    psum x2, waiting for transfers between devices, settle(): branch = lax.psum(partial_value.astype(jnp.bfloat16), 'tp')  67.9 us
    all_gather x1, waiting for transfers between devices, on_device(): full_down = lax.all_gather(w_down, 'fs', axis=1, tiled=True)  64.8 us
    all_gather x1, waiting for transfers between devices, on_device(): lax.all_gather(w_linear, 'fs', axis=0, tiled=True)  51.6 us
    all_gather x1, waiting for transfers between devices, on_device(): lax.all_gather(w_gated, 'fs', axis=0, tiled=True)  28.7 us
    all_gather x1, blocking collectives, on_device(): lax.all_gather(w_value, 'fs', axis=0, tiled=True)  26.9 us
    all_gather x1, blocking collectives, on_device(): lax.all_gather(w_outer_gate, 'fs', axis=0, tiled=True)  18 us
    all_gather x1, blocking collectives, on_device(): full_mix_out = lax.all_gather(w_mix_out, 'fs', axis=1, tiled=True)  15.3 us
    add x2, other arithmetic, conv_three(): taps[0] * padded[:, :-2] + taps[1] * padded[:, 1:-1]  8.51 us
  transfers between devices with their start and end apart: 6, of which 5 were waited for; matrix products, arithmetic and copies ran while one was open for 5% of the time, Pallas kernels for 0%

profile of v1, /device:TPU:0, one launch (start us, length us, event | category | flops | bytes accessed | tf_op | source)
XLA Modules:
  0.0 331.2 jit_solution(16020114559799785290)
XLA Ops:
  7.4 1.9 stack.2
  9.2 6.5 %all-to-all-start = ((bf16[4,384,192]{1,2,0:T(8,128)(2,1)}), bf16[4,384,192]{1,2,0:T(8,128)(2,1)S(1)}, u32[]{:S(2)}, u32[]{:S(2)}) async-start(bf16[4,384,192]{1,2,0:T(8,128)(2,1)} %stack.2), calls=%async_computation | async-start | bytes 1179648 | tf_op jit(solution)/shard_map/all_to_all | solution.py:13
  15.7 0.2 fusion.8
  16.0 26.9 %all_gather.19 = bf16[1536,192]{0,1:T(8,128)(2,1)S(1)} all-gather(bf16[384,192]{0,1:T(8,128)(2,1)S(1)} %copy-done.1), channel_id=1, replica_groups=mesh['rep'=2,'fs'=4,'tp'=4] {'fs'}, dimensions={0}, use_global_device_ids=true | all-gather | bytes 737280 | tf_op jit(solution)/shard_map/all_gather | solution.py:56
  42.9 18.0 %all_gather.18 = bf16[1536,192]{0,1:T(8,128)(2,1)S(1)} all-gather(bf16[384,192]{0,1:T(8,128)(2,1)S(1)} %copy-done.2), channel_id=1, replica_groups=mesh['rep'=2,'fs'=4,'tp'=4] {'fs'}, dimensions={0}, use_global_device_ids=true | all-gather | bytes 737280 | tf_op jit(solution)/shard_map/all_gather | solution.py:54
  60.9 15.3 %all_gather.20 = bf16[192,1536]{1,0:T(8,128)(2,1)S(1)} all-gather(bf16[192,384]{1,0:T(8,128)(2,1)S(1)} %copy-done.3), channel_id=1, replica_groups=mesh['rep'=2,'fs'=4,'tp'=4] {'fs'}, dimensions={1}, use_global_device_ids=true | all-gather | bytes 737280 | tf_op jit(solution)/shard_map/all_gather | solution.py:66
  76.2 0.1 copy.18
  76.3 0.5 fusion.18
  76.8 0.5 fusion.17
  77.3 0.1 reshape.64
  77.4 1.2 fusion.43
  78.6 2.1 convolution_convert_fusion.3
  80.8 0.0 all-gather.4.cloned.1.call-start
  80.8 0.5 all-gather.4.cloned.1.call-update
  81.4 0.0 all-gather.6.cloned.1.call-start
  81.4 0.5 all-gather.6.cloned.1.call-update
  81.9 0.0 all-gather.8.cloned.1.call-start
  82.0 0.5 all-gather.8.cloned.1.call-update
  82.5 0.0 all-reduce.7.cloned.1.call-start
  82.6 34.1 %all-reduce.5.cloned.1.call-done = bf16[256,1536]{1,0:T(8,128)(2,1)} async-done(((bf16[256,1536]{1,0:T(8,128)(2,1)}), bf16[256,1536]{1,0:T(8,128)(2,1)}) %all-reduce.5.cloned.1.call-update) | async-done | bytes 786448 | tf_op jit(solution)/shard_map/psum | solution.py:30
  116.8 1.4 fusion.4
  118.2 1.7 fusion.12
  119.8 28.7 %all-gather.4.cloned.1.call-done = bf16[1536,1056]{0,1:T(8,128)(2,1)} async-done(((bf16[384,1056]{0,1:T(8,128)(2,1)}), bf16[1536,1056]{0,1:T(8,128)(2,1)}) %all-gather.4.cloned.1.call-update) | async-done | bytes 3244048 | tf_op jit(solution)/shard_map/all_gather | solution.py:73
  148.5 4.0 %fusion.2 = f32[256,1056]{0,1:T(8,128)} fusion(bf16[1536,1056]{0,1:T(8,128)(2,1)} %all-gather.4.cloned.1.call-done, bf16[256,1536]{1,0:T(8,128)(2,1)S(1)} %get-tuple-element.9, f32[1536]{0:T(1024)S(1)} %copy-done.9, f32[256]{0:T(256)S(1)} %add_rsqrt_fusion.1), kind=kOutput, calls=%fused_computation.4 | convolution fusion | flops 832585728 | bytes 5118976 | tf_op jit(solution)/shard_map/dot_general | solution.py:76
  152.6 1.8 reshape.70
  154.4 7.3 %fusion.31 = f32[2,128,1056]{1,0,2:T(2,128)} fusion(f32[2,128,1056]{1,0,2:T(2,128)S(1)} %reshape.70, f32[1056]{0:T(1024)S(1)} %get-tuple-element.6, f32[1056]{0:T(1024)S(1)} %get-tuple-element.7, f32[1056]{0:T(1024)S(1)} %get-tuple-element.5), kind=kLoop, calls=%fused_computation.51 | loop fusion | flops 1351680 | bytes 2175360 | tf_op jit(solution)/shard_map/add | solution.py:25
  161.7 51.6 %all-gather.6.cloned.1.call-done = bf16[1536,1056]{0,1:T(8,128)(2,1)} async-done(((bf16[384,1056]{0,1:T(8,128)(2,1)}), bf16[1536,1056]{0,1:T(8,128)(2,1)}) %all-gather.6.cloned.1.call-update) | async-done | bytes 3244048 | tf_op jit(solution)/shard_map/all_gather | solution.py:72
  213.3 64.8 %all-gather.8.cloned.1.call-done = bf16[1056,1536]{1,0:T(8,128)(2,1)} async-done(((bf16[1056,384]{1,0:T(8,128)(2,1)}), bf16[1056,1536]{1,0:T(8,128)(2,1)}) %all-gather.8.cloned.1.call-update) | async-done | bytes 3244048 | tf_op jit(solution)/shard_map/all_gather | solution.py:83
  278.1 7.9 %convolution_convert_fusion.2 = bf16[256,1536]{1,0:T(8,128)(2,1)} fusion(bf16[1056,1536]{1,0:T(8,128)(2,1)} %all-gather.8.cloned.1.call-done, bf16[1536,1056]{0,1:T(8,128)(2,1)} %all-gather.6.cloned.1.call-done, f32[132,8,2,128]{3,2,1,0:T(2,128)} %bitcast.34, f32[1056]{0:T(1024)S(1)} %copy-done.10, bf16[256,1536]{1,0:T(8,128)(2,1)S(1)} %get-tuple-element.9, ...), kind=kOutput, calls=%fused_computation.6 | convolution fusion | flops 1666424832 | bytes 9153664 | tf_op jit(solution)/shard_map/dot_general | solution.py:84
  286.1 33.8 %all-reduce.7.cloned.1.call-done = bf16[256,1536]{1,0:T(8,128)(2,1)} async-done(((bf16[256,1536]{1,0:T(8,128)(2,1)}), bf16[256,1536]{1,0:T(8,128)(2,1)}) %all-reduce.7.cloned.1.call-update) | async-done | bytes 786448 | tf_op jit(solution)/shard_map/psum | solution.py:30
  319.9 1.4 fusion.6
  321.3 2.4 fusion.15
  (32 shorter events, 0.2 us)
Async XLA Ops:
  7.4 8.4 %copy-start = (bf16[256,1536]{1,0:T(8,128)(2,1)S(1)}, bf16[256,1536]{1,0:T(8,128)(2,1)}, u32[]{:S(2)}) copy-start(bf16[256,1536]{1,0:T(8,128)(2,1)} %param.15) | copy-start | bytes 2359300
  7.4 8.6 %copy-start.1 = (bf16[384,192]{0,1:T(8,128)(2,1)S(1)}, bf16[384,192]{0,1:T(8,128)(2,1)}, u32[]{:S(2)}) copy-start(bf16[384,192]{0,1:T(8,128)(2,1)} %param.19) | copy-start | bytes 442372
  7.4 35.6 %copy-start.2 = (bf16[384,192]{0,1:T(8,128)(2,1)S(1)}, bf16[384,192]{0,1:T(8,128)(2,1)}, u32[]{:S(2)}) copy-start(bf16[384,192]{0,1:T(8,128)(2,1)} %param.17) | copy-start | bytes 442372
  9.2 51.7 %copy-start.3 = (bf16[192,384]{1,0:T(8,128)(2,1)S(1)}, bf16[192,384]{1,0:T(8,128)(2,1)}, u32[]{:S(2)}) copy-start(bf16[192,384]{1,0:T(8,128)(2,1)} %param.21) | copy-start | bytes 442372
  9.2 67.0 %all-to-all-start = ((bf16[4,384,192]{1,2,0:T(8,128)(2,1)}), bf16[4,384,192]{1,2,0:T(8,128)(2,1)S(1)}, u32[]{:S(2)}, u32[]{:S(2)}) async-start(bf16[4,384,192]{1,2,0:T(8,128)(2,1)} %stack.2), calls=%async_computation | async-start | bytes 1179648 | tf_op jit(solution)/shard_map/all_to_all | solution.py:13
  15.7 60.5 %copy-start.7 = (f32[3,192]{1,0:T(4,128)S(1)}, f32[3,192]{1,0:T(4,128)}, u32[]{:S(2)}) copy-start(f32[3,192]{1,0:T(4,128)} %param.20) | copy-start | bytes 6916
  15.7 101.1 %all-reduce.5.cloned.1.call-start = ((), (), s32[]{:S(2)}) async-start(), calls=%async_computation.1 | async-start | bytes 1572864 | tf_op jit(solution)/shard_map/psum | solution.py:30
  16.0 60.3 %copy-start.8 = (f32[1536]{0:T(1024)S(1)}, f32[1536]{0:T(1024)}, u32[]{:S(2)}) copy-start(f32[1536]{0:T(1024)} %param.16) | copy-start | bytes 18436
  80.7 1.8 copy-start.4
  80.8 37.4 %copy-start.5 = (f32[1536]{0:T(1024)S(1)}, f32[1536]{0:T(1024)}, u32[]{:S(2)}) copy-start(f32[1536]{0:T(1024)} %param.22) | copy-start | bytes 18436
  80.8 67.7 %all-gather.4.cloned.1.call-start = ((), (), s32[]{:S(2)}) async-start(), calls=%async_computation.2 | async-start | bytes 4055040 | tf_op jit(solution)/shard_map/all_gather | solution.py:73
  81.4 132.0 %all-gather.6.cloned.1.call-start = ((), (), s32[]{:S(2)}) async-start(), calls=%async_computation.3 | async-start | bytes 4055040 | tf_op jit(solution)/shard_map/all_gather | solution.py:72
  81.9 196.2 %all-gather.8.cloned.1.call-start = ((), (), s32[]{:S(2)}) async-start(), calls=%async_computation.4 | async-start | bytes 4055040 | tf_op jit(solution)/shard_map/all_gather | solution.py:83
  82.5 237.4 %all-reduce.7.cloned.1.call-start = ((), (), s32[]{:S(2)}) async-start(), calls=%async_computation.5 | async-start | bytes 1572864 | tf_op jit(solution)/shard_map/psum | solution.py:30
  82.6 65.9 %copy-start.9 = (f32[1536]{0:T(1024)S(1)}, f32[1536]{0:T(1024)}, u32[]{:S(2)}) copy-start(f32[1536]{0:T(1024)} %param.23) | copy-start | bytes 18436
  154.4 123.7 %copy-start.10 = (f32[1056]{0:T(1024)S(1)}, f32[1056]{0:T(1024)}, u32[]{:S(2)}) copy-start(f32[1056]{0:T(1024)} %param.27) | copy-start | bytes 12676
  286.0 35.2 %copy-start.6 = (f32[1536]{0:T(1024)S(1)}, f32[1536]{0:T(1024)}, u32[]{:S(2)}) copy-start(f32[1536]{0:T(1024)} %param.29) | copy-start | bytes 18436
Sparse Core Ops, SparseCore 0:
  80.9 35.8 all-reduce.4
  286.2 33.6 all-reduce.6
Sparse Core Ops, SparseCore 1:
  82.9 65.6 all-gather.3
  150.0 63.3 all-gather.5
  214.8 63.3 all-gather.7
